TPU v7x, 32 devices: a whole 2x2x4 slice. The times are simulated.
32 devices in a mesh: ep: 8 (over z, x), tp: 4 (over y, core).
Axes of the slice: x: 2, y: 2, z: 4, core: 2. Of those that a mesh axis runs over, the one named last changes fastest.
Arguments:
- resid: bfloat16 [256, 2048], P('ep'), may hold values from -6 to 6
- norm_gain: bfloat16 [2048], replicated, may hold values from 0.099609375 to 1.8984375
- w_query: bfloat16 [2048, 1024], P(None, 'tp'), may hold values from -0.125 to 0.125
- w_key: bfloat16 [2048, 1024], P(None, 'tp'), may hold values from -0.125 to 0.125
- w_value: bfloat16 [2048, 1024], P(None, 'tp'), may hold values from -0.125 to 0.125
- w_gate: bfloat16 [2048, 1024], P(None, 'tp'), may hold values from -0.125 to 0.125
- head_gain: bfloat16 [1024], P('tp'), may hold values from 0.099609375 to 1.8984375
- w_output: bfloat16 [1024, 2048], P('tp'), may hold values from -0.1875 to 0.1875
- state: float32 [256, 8, 128, 128], P('ep', 'tp'), may hold values from -0.6 to 0.6
- positions: int32 [256], P('ep'), may hold values from 1024 to 8191
- ffn_gain: bfloat16 [2048], replicated, may hold values from 0.099609375 to 1.8984375
- w_mix: bfloat16 [2048], replicated, may hold values from -0.125 to 0.125
- dense_gate: bfloat16 [2048, 5632], P('tp', 'ep'), may hold values from -0.125 to 0.125
- dense_up: bfloat16 [2048, 5632], P('tp', 'ep'), may hold values from -0.125 to 0.125
- dense_down: bfloat16 [5632, 2048], P('ep', 'tp'), may hold values from -0.109375 to 0.109375
- routes: int32 [256, 2], P('ep'), may hold values from 0 to 7, all different within a row; in each aligned block of 32 rows (0 to 31, 32 to 63, ...) at most 16 rows name the same one
- route_weight: bfloat16 [256, 2], P('ep'), may hold values from 0.19921875 to 1
- expert_gate: bfloat16 [8, 2048, 4096], P('ep', None, 'tp'), may hold values from -0.125 to 0.125
- expert_up: bfloat16 [8, 2048, 4096], P('ep', None, 'tp'), may hold values from -0.125 to 0.125
- expert_down: bfloat16 [8, 4096, 2048], P('ep', 'tp'), may hold values from -0.09375 to 0.09375
Outputs:
- final: bfloat16 [256, 2048], P('ep', 'tp')
- new_state: float32 [256, 8, 128, 128], P('ep', 'tp')
Inputs may be any that keep to these rules, and one draw needn't show every extreme that they name: `routes`: each row names 2 different experts; in the rows of one index of ep no expert is named by more than 16 rows, a bound that some block reaches; every expert is named by some row.
All inputs are finite; a program needn't handle non-finite values.
Results may differ from a plain program's by a relative error of at most 0.018.
Values may be sent and summed in bfloat16 or wider, within the bound.
A program may use at most 64 MiB of HBM per device.

v0:
```python
import jax
import jax.numpy as jnp
from jax import lax
from jax.sharding import PartitionSpec as P

EPSILON = 1e-06
THETA = 10000.0


def rms_norm(inputs, scaling):
    square = jnp.mean(inputs * inputs, axis=-1, keepdims=True)
    return inputs * lax.rsqrt(square + EPSILON) * scaling.astype(jnp.float32)


def rotate(inputs, places):
    halfway = inputs.shape[-1] // 2
    inverse = THETA ** (-jnp.arange(halfway, dtype=jnp.float32) / halfway)
    angles = places.astype(jnp.float32)[:, None] * inverse[None, :]
    cosine = jnp.cos(angles)[:, None, :]
    sine_of = jnp.sin(angles)[:, None, :]
    former = inputs[..., :halfway]
    latter = inputs[..., halfway:]
    return jnp.concatenate(
        [former * cosine - latter * sine_of, former * sine_of + latter * cosine], axis=-1
    )


def retain(queries, keys_in, values_in, gating, memory, places, head_first, head_gain):
    seqs_here = queries.shape[0]
    heads_here = memory.shape[1]
    head_size = memory.shape[2]
    head_shape = (seqs_here, heads_here, head_size)
    query_rot = rotate(queries.astype(jnp.float32).reshape(head_shape), places)
    key_rot = rotate(keys_in.astype(jnp.float32).reshape(head_shape), places) * head_size ** (-0.5)
    value_heads = values_in.astype(jnp.float32).reshape(head_shape)
    head_index = head_first + jnp.arange(heads_here, dtype=jnp.float32)
    decays = 1.0 - jnp.exp2(-1.0 - 1.5 * head_index)
    within = jnp.sum(query_rot * key_rot, axis=-1, keepdims=True) * value_heads
    carried = (
        jnp.einsum("shd,shde->she", query_rot, memory, precision=lax.Precision.HIGHEST)
        * decays[None, :, None]
    )
    mixture = within + carried
    new_memory = (
        decays[None, :, None, None] * memory + key_rot[:, :, :, None] * value_heads[:, :, None, :]
    )
    centre = jnp.mean(mixture, axis=-1, keepdims=True)
    spread = jnp.mean(jnp.square(mixture - centre), axis=-1, keepdims=True)
    normed = ((mixture - centre) * lax.rsqrt(spread + EPSILON)).reshape(
        seqs_here, heads_here * head_size
    )
    normed = normed * head_gain.astype(jnp.float32)
    output = (jax.nn.silu(gating.astype(jnp.float32)) * normed).astype(jnp.bfloat16)
    return (output, new_memory)


def expert_hidden(chosen, gate_weight, up_weight):
    gate_value = jnp.dot(chosen, gate_weight, preferred_element_type=jnp.float32)
    up_value = jnp.dot(chosen, up_weight, preferred_element_type=jnp.float32)
    return (jax.nn.silu(gate_value) * up_value).astype(jnp.bfloat16)


def padded_experts(
    normed_mid, routes, route_weight, expert_gate, expert_up, expert_down, capacity, experts_all
):
    seq_dev, model_width = normed_mid.shape
    top_count = routes.shape[1]
    flat_ids = routes.reshape(-1)
    expert_ids = jnp.arange(experts_all, dtype=jnp.int32)
    onehot = (flat_ids[:, None] == expert_ids[None, :]).astype(jnp.int32)
    ranks = jnp.sum((jnp.cumsum(onehot, axis=0) - 1) * onehot, axis=1)
    slot_ids = flat_ids * capacity + ranks
    slot_range = jnp.arange(experts_all * capacity, dtype=jnp.int32)
    dispatch = (slot_range[:, None] == slot_ids[None, :]).astype(jnp.bfloat16)
    repeated = jnp.repeat(normed_mid, top_count, axis=0)
    outgoing = jnp.dot(dispatch, repeated, preferred_element_type=jnp.float32).astype(jnp.bfloat16)
    outgoing = outgoing.reshape(experts_all, capacity, model_width)
    arrived = lax.all_to_all(outgoing, "ep", split_axis=0, concat_axis=0, tiled=True)
    sources = arrived.shape[0]
    items = arrived.shape[1]
    hidden_e = expert_hidden(
        arrived.reshape(sources * items, model_width), expert_gate[0], expert_up[0]
    )
    partial_value = jnp.dot(hidden_e, expert_down[0], preferred_element_type=jnp.float32)
    summed = lax.psum_scatter(
        partial_value.astype(jnp.bfloat16), "tp", scatter_dimension=1, tiled=True
    )
    returned = lax.all_to_all(
        summed.reshape(sources, items, summed.shape[1]),
        "ep",
        split_axis=0,
        concat_axis=0,
        tiled=True,
    )
    flat_back = returned.reshape(experts_all * capacity, returned.shape[2])
    weighted = flat_back[slot_ids].astype(jnp.float32) * route_weight.reshape(-1)[:, None].astype(
        jnp.float32
    )
    return jnp.sum(weighted.reshape(seq_dev, top_count, weighted.shape[1]), axis=1)


def per_device(
    resid,
    norm_gain,
    w_query,
    w_key,
    w_value,
    w_gate,
    head_gain,
    w_output,
    state,
    positions,
    ffn_gain,
    w_mix,
    dense_gate,
    dense_up,
    dense_down,
    routes,
    route_weight,
    expert_gate,
    expert_up,
    expert_down,
):
    seq_dev = resid.shape[0]
    model_width = resid.shape[1]
    tp_count = lax.axis_size("tp")
    ep_count = lax.axis_size("ep")
    model_tp = model_width // tp_count
    tp_index = lax.axis_index("tp")
    normed_in = rms_norm(resid.astype(jnp.float32), norm_gain).astype(jnp.bfloat16)

    def project(weight):
        return jnp.dot(normed_in, weight, preferred_element_type=jnp.float32).astype(jnp.bfloat16)

    heads_here = state.shape[1]
    head_first = (tp_index * heads_here).astype(jnp.float32)
    retained, new_state = retain(
        project(w_query),
        project(w_key),
        project(w_value),
        project(w_gate),
        state,
        positions,
        head_first,
        head_gain,
    )
    partial_value = jnp.dot(retained, w_output, preferred_element_type=jnp.float32)
    attention = lax.psum(partial_value.astype(jnp.bfloat16), "tp").astype(jnp.float32)
    middle = resid.astype(jnp.float32) + attention
    normed_mid = rms_norm(middle, ffn_gain).astype(jnp.bfloat16)
    mixing = jax.nn.sigmoid(jnp.dot(normed_mid, w_mix[:, None], preferred_element_type=jnp.float32))

    def own_columns(matrix):
        return lax.dynamic_slice_in_dim(matrix, tp_index * model_tp, model_tp, 1)

    top_count = routes.shape[1]
    capacity = max(2, 2 * seq_dev * top_count // ep_count)
    dense_rows = lax.all_gather(own_columns(normed_mid), "ep", axis=0, tiled=True)
    moe_out = padded_experts(
        normed_mid, routes, route_weight, expert_gate, expert_up, expert_down, capacity, ep_count
    )
    gate_part = jnp.dot(dense_rows, dense_gate, preferred_element_type=jnp.float32)
    up_part = jnp.dot(dense_rows, dense_up, preferred_element_type=jnp.float32)
    gate_sum, up_sum = (
        lax.psum(gate_part.astype(jnp.bfloat16), "tp").astype(jnp.float32),
        lax.psum(up_part.astype(jnp.bfloat16), "tp").astype(jnp.float32),
    )
    dense_hidden = (jax.nn.silu(gate_sum) * up_sum).astype(jnp.bfloat16)
    dense_out = lax.psum_scatter(
        jnp.dot(dense_hidden, dense_down, preferred_element_type=jnp.float32).astype(jnp.bfloat16),
        "ep",
        scatter_dimension=0,
        tiled=True,
    ).astype(jnp.float32)
    final = (own_columns(middle) + moe_out + mixing * dense_out).astype(jnp.bfloat16)
    return (final, new_state)


def solution(mesh):
    in_specs = (
        P("ep", None),
        P(),
        P(None, "tp"),
        P(None, "tp"),
        P(None, "tp"),
        P(None, "tp"),
        P("tp"),
        P("tp", None),
        P("ep", "tp", None, None),
        P("ep"),
        P(),
        P(),
        P("tp", "ep"),
        P("tp", "ep"),
        P("ep", "tp"),
        P("ep", None),
        P("ep", None),
        P("ep", None, "tp"),
        P("ep", None, "tp"),
        P("ep", "tp", None),
    )
    out_specs = (P("ep", "tp"), P("ep", "tp", None, None))
    return jax.shard_map(
        per_device, mesh=mesh, in_specs=in_specs, out_specs=out_specs, check_vma=False
    )
```

profile of v0, /device:TPU:0, one launch (start us, length us, event | category | flops | bytes accessed | tf_op | source)
XLA Modules:
  0.0 234.7 jit_solution(9448984096883275482)
XLA Ops:
  8.0 1.0 fusion.40
  10.4 1.6 fusion.20
  12.1 1.7 fusion.19
  13.8 1.6 fusion.18
  16.0 5.3 %fusion.61 = f32[32,2,1,128]{3,2,1,0:T(1,128)S(1)} fusion(f32[32,2,128,1]{2,3,1,0:T(1,128)S(1)} %bitcast.72, f32[32,2,128,128]{3,2,1,0:T(8,128)} %param.28), kind=kOutput, calls=%fused_computation.95 | convolution fusion | flops 12582912 | bytes 4259840 | tf_op jit(solution)/shard_map/shd,shde->she/dot_general | solution.py:40
  21.9 1.5 convolution_convert_fusion.1
  24.0 34.1 %all-reduce.4.cloned.1.call-done = bf16[32,2048]{1,0:T(8,128)(2,1)} async-done(((bf16[32,2048]{1,0:T(8,128)(2,1)}), bf16[32,2048]{1,0:T(8,128)(2,1)}) %all-reduce.4.cloned.1.call-update) | async-done | bytes 131088 | tf_op jit(solution)/shard_map/psum | solution.py:148
  58.1 1.1 convert_add_fusion
  59.1 1.0 multiply_convert_fusion
  60.4 1.1 convolution_convert_fusion
  61.5 5.5 %all-to-all-start = ((bf16[8,16,2048]{2,1,0:T(8,128)(2,1)}), bf16[8,16,2048]{2,1,0:T(8,128)(2,1)S(1)}, u32[]{:S(2)}, u32[]{:S(2)}) async-start(bf16[8,16,2048]{2,1,0:T(8,128)(2,1)} %bitcast.4), calls=%async_computation | async-start | bytes 1048576 | tf_op jit(solution)/shard_map/all_to_all | solution.py:78
  67.0 36.6 %all_gather.3 = bf16[256,512]{1,0:T(8,128)(2,1)S(1)} all-gather(bf16[32,512]{1,0:T(8,128)(2,1)S(1)} %constant_dynamic-slice_fusion), channel_id=1, replica_groups=mesh['ep'=8,'tp'=4] {'ep'}, dimensions={0}, use_global_device_ids=true | all-gather | bytes 294912 | tf_op jit(solution)/shard_map/all_gather | solution.py:158
  103.7 1.1 convolution_convert_fusion.2
  104.8 1.1 convolution_convert_fusion.3
  106.0 2.9 %fusion.5 = f32[128,1024]{1,0:T(8,128)S(1)} fusion(bf16[128,2048]{1,0:T(8,128)(2,1)S(1)} %bitcast.69, bf16[1,2048,1024]{2,1,0:T(8,128)(2,1)} %param.37), kind=kOutput, calls=%fused_computation.6 | convolution fusion | flops 536870912 | bytes 5242880 | tf_op jit(solution)/shard_map/dot_general | solution.py:58
  109.0 5.6 %fusion.7 = bf16[128,2048]{1,0:T(8,128)(2,1)} fusion(bf16[1,1024,2048]{2,1,0:T(8,128)(2,1)} %param.39, bf16[128,2048]{1,0:T(8,128)(2,1)S(1)} %bitcast.70, bf16[1,2048,1024]{2,1,0:T(8,128)(2,1)} %param.38, f32[128,1024]{1,0:T(8,128)S(1)} %fusion.5), kind=kOutput, calls=%fused_computation.9 | convolution fusion | flops 1074790400 | bytes 9961472 | tf_op jit(solution)/shard_map/dot_general | solution.py:84
  114.9 4.3 %multiply_add_fusion = f32[32,2,128,128]{3,2,1,0:T(8,128)} fusion(f32[32,2,128,128]{3,2,1,0:T(8,128)} %param.28, f32[32,2,128]{2,1,0:T(2,128)S(1)} %copy-done.6, f32[32,2,128]{2,1,0:T(2,128)S(1)} %copy-done.8, f32[2]{0:T(128)S(1)} %exponential_subtract_fusion), kind=kLoop, calls=%fused_computation.8 | loop fusion | flops 3145728 | bytes 8454152 | tf_op jit(solution)/shard_map/add | solution.py:45
  119.2 18.0 %all-reduce.6.cloned.1.call-done = (bf16[256,704]{0,1:T(8,128)(2,1)}, bf16[256,704]{0,1:T(8,128)(2,1)}) async-done(((bf16[256,704]{0,1:T(8,128)(2,1)}, bf16[256,704]{0,1:T(8,128)(2,1)}), (bf16[256,704]{0,1:T(8,128)(2,1)}, bf16[256,704]{0,1:T(8,128)(2,1)})) %all-reduce.6.cloned.1.call-update) | async-done | bytes 720912 | tf_op jit(solution)/shard_map/psum | solution.py:166
  137.2 2.2 convolution_convert_fusion.4
  139.5 21.9 %reduce-scatter.3.cloned.1.call-done = bf16[128,512]{1,0:T(8,128)(2,1)} async-done(((bf16[128,2048]{1,0:T(8,128)(2,1)}), bf16[128,512]{1,0:T(8,128)(2,1)}) %reduce-scatter.3.cloned.1.call-update) | async-done | bytes 131088 | tf_op jit(solution)/shard_map/reduce_scatter | solution.py:85
  161.4 5.5 %all-to-all-start.1 = ((bf16[8,16,512]{2,1,0:T(8,128)(2,1)}), bf16[8,16,512]{2,1,0:T(8,128)(2,1)S(1)}, u32[]{:S(2)}, u32[]{:S(2)}) async-start(bf16[8,16,512]{2,1,0:T(8,128)(2,1)} %bitcast.73), calls=%async_computation.2 | async-start | bytes 262144 | tf_op jit(solution)/shard_map/all_to_all | solution.py:88
  167.2 7.1 %all-to-all-done.1 = bf16[8,16,512]{2,1,0:T(8,128)(2,1)S(1)} async-done(((bf16[8,16,512]{2,1,0:T(8,128)(2,1)}), bf16[8,16,512]{2,1,0:T(8,128)(2,1)S(1)}, u32[]{:S(2)}, u32[]{:S(2)}) %all-to-all-start.1) | async-done | bytes 131104 | tf_op jit(solution)/shard_map/all_to_all | solution.py:88
  175.3 51.4 %reduce-scatter.5.cloned.1.call-done = bf16[32,512]{1,0:T(8,128)(2,1)} async-done(((bf16[256,512]{1,0:T(8,128)(2,1)}), bf16[32,512]{1,0:T(8,128)(2,1)}) %reduce-scatter.5.cloned.1.call-update) | async-done | bytes 32784 | tf_op jit(solution)/shard_map/reduce_scatter | solution.py:169
  226.7 1.4 add_convert_fusion
  (76 shorter events, 5.8 us)
Async XLA Ops:
  7.2 14.7 %copy-start = (bf16[256,2048]{1,0:T(8,128)(2,1)S(1)}, bf16[256,2048]{1,0:T(8,128)(2,1)}, u32[]{:S(2)}) copy-start(bf16[256,2048]{1,0:T(8,128)(2,1)} %param.27) | copy-start | bytes 3145732
  7.2 50.9 %all-reduce.4.cloned.1.call-start = ((), (), s32[]{:S(2)}) async-start(), calls=%async_computation.4 | async-start | bytes 262144 | tf_op jit(solution)/shard_map/psum | solution.py:148
  12.0 9.9 %copy-start.1 = (bf16[32,2048]{1,0:T(8,128)(2,1)S(1)}, bf16[32,2048]{1,0:T(8,128)(2,1)}, u32[]{:S(2)}) copy-start(bf16[32,2048]{1,0:T(8,128)(2,1)} %param.20) | copy-start | bytes 393220
  12.0 9.9 %copy-start.2 = (bf16[2048,256]{1,0:T(8,128)(2,1)S(1)}, bf16[2048,256]{1,0:T(8,128)(2,1)}, u32[]{:S(2)}) copy-start(bf16[2048,256]{1,0:T(8,128)(2,1)} %param.25) | copy-start | bytes 3145732
  15.4 8.0 %copy-start.11 = (s32[32,2]{0,1:T(2,128)S(1)}, s32[32,2]{0,1:T(2,128)}, u32[]{:S(2)}) copy-start(s32[32,2]{0,1:T(2,128)} %param.35) | copy-start | bytes 772
  15.5 8.5 %copy-start.9 = (bf16[2048]{0:T(1024)(128)(2,1)S(1)}, bf16[2048]{0:T(1024)(128)(2,1)}, u32[]{:S(2)}) copy-start(bf16[2048]{0:T(1024)(128)(2,1)} %param.30) | copy-start | bytes 12292
  15.5 6.0 %copy-start.5 = (f32[32,2,128]{2,1,0:T(2,128)}, f32[32,2,128]{2,1,0:T(2,128)S(1)}, u32[]{:S(2)}) copy-start(f32[32,2,128]{2,1,0:T(2,128)S(1)} %reshape.238) | copy-start | bytes 98308
  16.0 5.9 %copy-start.7 = (f32[32,2,128]{2,1,0:T(2,128)}, f32[32,2,128]{2,1,0:T(2,128)S(1)}, u32[]{:S(2)}) copy-start(f32[32,2,128]{2,1,0:T(2,128)S(1)} %get-tuple-element.17) | copy-start | bytes 98308
  21.3 82.4 %copy-start.3 = (bf16[512,704]{0,1:T(8,128)(2,1)S(1)}, bf16[512,704]{0,1:T(8,128)(2,1)}, u32[]{:S(2)}) copy-start(bf16[512,704]{0,1:T(8,128)(2,1)} %param.33) | copy-start | bytes 2162692
  23.4 81.5 %copy-start.4 = (bf16[512,704]{0,1:T(8,128)(2,1)S(1)}, bf16[512,704]{0,1:T(8,128)(2,1)}, u32[]{:S(2)}) copy-start(bf16[512,704]{0,1:T(8,128)(2,1)} %param.32) | copy-start | bytes 2162692
  61.5 44.6 %all-to-all-start = ((bf16[8,16,2048]{2,1,0:T(8,128)(2,1)}), bf16[8,16,2048]{2,1,0:T(8,128)(2,1)S(1)}, u32[]{:S(2)}, u32[]{:S(2)}) async-start(bf16[8,16,2048]{2,1,0:T(8,128)(2,1)} %bitcast.4), calls=%async_computation | async-start | bytes 1048576 | tf_op jit(solution)/shard_map/all_to_all | solution.py:78
  67.0 70.2 %all-reduce.6.cloned.1.call-start = ((), (), s32[]{:S(2)}) async-start(), calls=%async_computation.7 | async-start | bytes 1441792 | tf_op jit(solution)/shard_map/psum | solution.py:166
  106.0 55.4 %reduce-scatter.3.cloned.1.call-start = ((), (), s32[]{:S(2)}) async-start(), calls=%async_computation.5 | async-start | bytes 655360 | tf_op jit(solution)/shard_map/reduce_scatter | solution.py:85
  109.0 5.9 %copy-start.6 = (f32[32,2,128]{2,1,0:T(2,128)S(1)}, f32[32,2,128]{2,1,0:T(2,128)}, u32[]{:S(2)}) copy-start(f32[32,2,128]{2,1,0:T(2,128)} %copy-done.5) | copy-start | bytes 98308
  109.0 5.9 %copy-start.8 = (f32[32,2,128]{2,1,0:T(2,128)S(1)}, f32[32,2,128]{2,1,0:T(2,128)}, u32[]{:S(2)}) copy-start(f32[32,2,128]{2,1,0:T(2,128)} %copy-done.7) | copy-start | bytes 98308
  114.6 112.0 %reduce-scatter.5.cloned.1.call-start = ((), (), s32[]{:S(2)}) async-start(), calls=%async_computation.6 | async-start | bytes 294912 | tf_op jit(solution)/shard_map/reduce_scatter | solution.py:169
  114.9 22.3 %copy-start.13 = (bf16[704,512]{1,0:T(8,128)(2,1)S(1)}, bf16[704,512]{1,0:T(8,128)(2,1)}, u32[]{:S(2)}) copy-start(bf16[704,512]{1,0:T(8,128)(2,1)} %param.34) | copy-start | bytes 2162692
  119.2 47.7 %copy-start.10 = (bf16[2048]{0:T(1024)(128)(2,1)S(1)}, bf16[2048]{0:T(1024)(128)(2,1)}, u32[]{:S(2)}) copy-start(bf16[2048]{0:T(1024)(128)(2,1)} %param.31) | copy-start | bytes 12292
  119.2 47.7 %copy-start.12 = (bf16[32,2]{0,1:T(2,128)(2,1)S(1)}, bf16[32,2]{0,1:T(2,128)(2,1)}, u32[]{:S(2)}) copy-start(bf16[32,2]{0,1:T(2,128)(2,1)} %param.36) | copy-start | bytes 388
  161.4 12.9 %all-to-all-start.1 = ((bf16[8,16,512]{2,1,0:T(8,128)(2,1)}), bf16[8,16,512]{2,1,0:T(8,128)(2,1)S(1)}, u32[]{:S(2)}, u32[]{:S(2)}) async-start(bf16[8,16,512]{2,1,0:T(8,128)(2,1)} %bitcast.73), calls=%async_computation.2 | async-start | bytes 262144 | tf_op jit(solution)/shard_map/all_to_all | solution.py:88
Sparse Core Ops, SparseCore 0:
  23.5 34.4 all-reduce.3
  106.1 31.0 all-reduce.5
  139.7 21.6 reduce-scatter.2
  164.6 62.0 reduce-scatter.4
where the time goes:
time: 235 us
  waiting for transfers between devices  132 us (56%)
  blocking collectives  36.6 us (16%)
  matrix products  26 us (11%)
  between operations  14.2 us (6%)
  other arithmetic  12.6 us (5%)
  starting transfers between devices  11.2 us (5%)
    reduce_scatter x1, waiting for transfers between devices, per_device(): lax.psum_scatter(jnp.dot(dense_hidden, dense_down, preferred_element_type...  51.4 us
    all_gather x1, blocking collectives, per_device(): lax.all_gather(own_columns(normed_mid), 'ep', axis=0, tiled=True)  36.6 us
    psum x1, waiting for transfers between devices, per_device(): lax.psum(partial_value.astype(jnp.bfloat16), 'tp').astype(jnp.float32)  34.1 us
    reduce_scatter x1, waiting for transfers between devices, padded_experts(): lax.psum_scatter(partial_value.astype(jnp.bfloat16), 'tp', scatter_dimens...  21.9 us
    psum x1, waiting for transfers between devices, per_device(): lax.psum(up_part.astype(jnp.bfloat16), 'tp').astype(jnp.float32)  18 us
    all_to_all x1, waiting for transfers between devices, padded_experts(): lax.all_to_all(summed.reshape(sources, items, summed.shape[1]), 'ep', spl...  7.07 us
    dot_general x1, matrix products, padded_experts(): jnp.dot(hidden_e, expert_down[0], preferred_element_type=jnp.float32)  5.62 us
    all_to_all x1, starting transfers between devices, padded_experts(): lax.all_to_all(summed.reshape(sources, items, summed.shape[1]), 'ep', spl...  5.51 us
  transfers between devices with their start and end apart: 6, of which 5 were waited for; matrix products, arithmetic and copies ran while one was open for 8% of the time, Pallas kernels for 0%

commit v1 on v0

--- a/solution.py
+++ b/solution.py
@@ -5,6 +5,11 @@
 
 EPSILON = 1e-06
 THETA = 10000.0
+
+
+def summed_here(x, mesh_axis):
+    parts = lax.all_gather(x, mesh_axis)
+    return jnp.sum(parts, axis=0)
 
 
 def rms_norm(inputs, scaling):
@@ -145,7 +150,7 @@
         head_gain,
     )
     partial_value = jnp.dot(retained, w_output, preferred_element_type=jnp.float32)
-    attention = lax.psum(partial_value.astype(jnp.bfloat16), "tp").astype(jnp.float32)
+    attention = summed_here(partial_value.astype(jnp.bfloat16), "tp").astype(jnp.float32)
     middle = resid.astype(jnp.float32) + attention
     normed_mid = rms_norm(middle, ffn_gain).astype(jnp.bfloat16)
     mixing = jax.nn.sigmoid(jnp.dot(normed_mid, w_mix[:, None], preferred_element_type=jnp.float32))

time: 235 us -> 212 us (0.902)
  waiting for transfers between devices: 132 us -> 98.7 us
  blocking collectives: 36.6 us -> 46.8 us
    psum x1 -> x0, waiting for transfers between devices: 34.1 us -> none  [per_device(): lax.psum(partial_value.astype(jnp.bfloat16), 'tp').astype(jnp.float32)]
    all_gather x0 -> x1, blocking collectives: none -> 8.81 us  [summed_here(): parts = lax.all_gather(x, mesh_axis)]
  transfers between devices with their start and end apart: 6 -> 5, of which waited for: 5 -> 4; matrix products, arithmetic and copies ran while one was open for 8% -> 9% of each run, Pallas kernels for 0% -> 0%
where the time goes in v1:
time: 212 us; the launch traced here: 211 us
  waiting for transfers between devices  98.7 us (47%)
  blocking collectives  46.8 us (22%)
  matrix products  25.9 us (12%)
  between operations  14.1 us (7%)
  other arithmetic  12.2 us (6%)
  starting transfers between devices  11.4 us (5%)
  local copies, waits for them, and re-layouts  2.34 us (1%)
    reduce_scatter x1, waiting for transfers between devices, per_device(): lax.psum_scatter(jnp.dot(dense_hidden, dense_down, preferred_element_type...  51.5 us
    all_gather x1, blocking collectives, per_device(): lax.all_gather(own_columns(normed_mid), 'ep', axis=0, tiled=True)  38 us
    reduce_scatter x1, waiting for transfers between devices, padded_experts(): lax.psum_scatter(partial_value.astype(jnp.bfloat16), 'tp', scatter_dimens...  21.9 us
    psum x1, waiting for transfers between devices, per_device(): lax.psum(up_part.astype(jnp.bfloat16), 'tp').astype(jnp.float32)  18.2 us
    all_gather x1, blocking collectives, summed_here(): parts = lax.all_gather(x, mesh_axis)  8.81 us
    all_to_all x1, waiting for transfers between devices, padded_experts(): lax.all_to_all(summed.reshape(sources, items, summed.shape[1]), 'ep', spl...  7.08 us
    all_to_all x1, starting transfers between devices, padded_experts(): lax.all_to_all(outgoing, 'ep', split_axis=0, concat_axis=0, tiled=True)  5.81 us
    dot_general x1, matrix products, padded_experts(): jnp.dot(hidden_e, expert_down[0], preferred_element_type=jnp.float32)  5.62 us
  transfers between devices with their start and end apart: 5, of which 4 were waited for; matrix products, arithmetic and copies ran while one was open for 9% of the time, Pallas kernels for 0%

profile of v1, /device:TPU:0, one launch (start us, length us, event | category | flops | bytes accessed | tf_op | source)
XLA Modules:
  0.0 211.5 jit_solution(18385367670551576829)
XLA Ops:
  7.2 0.7 convert_element_type.113
  8.0 1.0 fusion.40
  11.1 0.8 copy.25
  12.9 1.6 fusion.20
  14.6 1.7 fusion.19
  16.3 1.6 fusion.18
  18.4 5.3 %fusion.61 = f32[32,2,1,128]{3,2,1,0:T(1,128)S(1)} fusion(f32[32,2,128,1]{2,3,1,0:T(1,128)S(1)} %bitcast.74, f32[32,2,128,128]{3,2,1,0:T(8,128)} %param.28), kind=kOutput, calls=%fused_computation.95 | convolution fusion | flops 12582912 | bytes 4259840 | tf_op jit(solution)/shard_map/shd,shde->she/dot_general | solution.py:45
  24.4 0.8 convolution_convert_fusion.1
  25.2 8.8 %all-gather = bf16[128,2048]{1,0:T(8,128)(2,1)S(1)} all-gather(bf16[32,2048]{1,0:T(8,128)(2,1)S(1)} %convolution_convert_fusion.1), channel_id=2, replica_groups=mesh['ep'=8,'tp'=4] {'tp'}, dimensions={0}, use_global_device_ids=true | all-gather | bytes 655360 | tf_op jit(solution)/shard_map/all_gather | solution.py:11
  34.6 1.8 convolution_convert_fusion
  36.3 5.8 %all-to-all-start = ((bf16[8,16,2048]{2,1,0:T(8,128)(2,1)}), bf16[8,16,2048]{2,1,0:T(8,128)(2,1)S(1)}, u32[]{:S(2)}, u32[]{:S(2)}) async-start(bf16[8,16,2048]{2,1,0:T(8,128)(2,1)} %bitcast.5), calls=%async_computation | async-start | bytes 1048576 | tf_op jit(solution)/shard_map/all_to_all | solution.py:83
  42.2 38.0 %all_gather.11 = bf16[256,512]{1,0:T(8,128)(2,1)S(1)} all-gather(bf16[32,512]{1,0:T(8,128)(2,1)S(1)} %constant_dynamic-slice_fusion), channel_id=1, replica_groups=mesh['ep'=8,'tp'=4] {'ep'}, dimensions={0}, use_global_device_ids=true | all-gather | bytes 294912 | tf_op jit(solution)/shard_map/all_gather | solution.py:163
  80.2 1.1 convolution_convert_fusion.2
  81.3 1.1 convolution_convert_fusion.3
  82.5 2.9 %fusion.5 = f32[128,1024]{1,0:T(8,128)S(1)} fusion(bf16[128,2048]{1,0:T(8,128)(2,1)S(1)} %bitcast.70, bf16[1,2048,1024]{2,1,0:T(8,128)(2,1)} %param.37), kind=kOutput, calls=%fused_computation.6 | convolution fusion | flops 536870912 | bytes 5242880 | tf_op jit(solution)/shard_map/dot_general | solution.py:63
  85.5 5.6 %fusion.7 = bf16[128,2048]{1,0:T(8,128)(2,1)} fusion(bf16[1,1024,2048]{2,1,0:T(8,128)(2,1)} %param.39, bf16[128,2048]{1,0:T(8,128)(2,1)S(1)} %bitcast.71, bf16[1,2048,1024]{2,1,0:T(8,128)(2,1)} %param.38, f32[128,1024]{1,0:T(8,128)S(1)} %fusion.5), kind=kOutput, calls=%fused_computation.9 | convolution fusion | flops 1074790400 | bytes 9961472 | tf_op jit(solution)/shard_map/dot_general | solution.py:89
  91.4 4.3 %multiply_add_fusion = f32[32,2,128,128]{3,2,1,0:T(8,128)} fusion(f32[32,2,128,128]{3,2,1,0:T(8,128)} %param.28, f32[32,2,128]{2,1,0:T(2,128)S(1)} %copy-done.6, f32[32,2,128]{2,1,0:T(2,128)S(1)} %copy-done.8, f32[2]{0:T(128)S(1)} %exponential_subtract_fusion), kind=kLoop, calls=%fused_computation.8 | loop fusion | flops 3145728 | bytes 8454152 | tf_op jit(solution)/shard_map/add | solution.py:50
  95.7 18.2 %all-reduce.3.cloned.1.call-done = (bf16[256,704]{0,1:T(8,128)(2,1)}, bf16[256,704]{0,1:T(8,128)(2,1)}) async-done(((bf16[256,704]{0,1:T(8,128)(2,1)}, bf16[256,704]{0,1:T(8,128)(2,1)}), (bf16[256,704]{0,1:T(8,128)(2,1)}, bf16[256,704]{0,1:T(8,128)(2,1)})) %all-reduce.3.cloned.1.call-update) | async-done | bytes 720912 | tf_op jit(solution)/shard_map/psum | solution.py:171
  113.9 2.2 %convolution_convert_fusion.4 = bf16[256,512]{1,0:T(8,128)(2,1)} fusion(bf16[704,512]{1,0:T(8,128)(2,1)S(1)} %copy-done.12, bf16[256,704]{0,1:T(8,128)(2,1)} %get-tuple-element.2, bf16[256,704]{0,1:T(8,128)(2,1)} %get-tuple-element.3), kind=kOutput, calls=%fused_computation.16 | convolution fusion | flops 186122240 | bytes 1703936 | tf_op jit(solution)/shard_map/dot_general | solution.py:175
  116.2 21.9 %reduce-scatter.3.cloned.1.call-done = bf16[128,512]{1,0:T(8,128)(2,1)} async-done(((bf16[128,2048]{1,0:T(8,128)(2,1)}), bf16[128,512]{1,0:T(8,128)(2,1)}) %reduce-scatter.3.cloned.1.call-update) | async-done | bytes 131088 | tf_op jit(solution)/shard_map/reduce_scatter | solution.py:90
  138.1 5.5 %all-to-all-start.1 = ((bf16[8,16,512]{2,1,0:T(8,128)(2,1)}), bf16[8,16,512]{2,1,0:T(8,128)(2,1)S(1)}, u32[]{:S(2)}, u32[]{:S(2)}) async-start(bf16[8,16,512]{2,1,0:T(8,128)(2,1)} %bitcast.75), calls=%async_computation.2 | async-start | bytes 262144 | tf_op jit(solution)/shard_map/all_to_all | solution.py:93
  143.9 7.1 %all-to-all-done.1 = bf16[8,16,512]{2,1,0:T(8,128)(2,1)S(1)} async-done(((bf16[8,16,512]{2,1,0:T(8,128)(2,1)}), bf16[8,16,512]{2,1,0:T(8,128)(2,1)S(1)}, u32[]{:S(2)}, u32[]{:S(2)}) %all-to-all-start.1) | async-done | bytes 131104 | tf_op jit(solution)/shard_map/all_to_all | solution.py:93
  152.0 51.5 %reduce-scatter.5.cloned.1.call-done = bf16[32,512]{1,0:T(8,128)(2,1)} async-done(((bf16[256,512]{1,0:T(8,128)(2,1)}), bf16[32,512]{1,0:T(8,128)(2,1)}) %reduce-scatter.5.cloned.1.call-update) | async-done | bytes 32784 | tf_op jit(solution)/shard_map/reduce_scatter | solution.py:174
  203.5 1.4 add_convert_fusion
  (73 shorter events, 6.5 us)
Async XLA Ops:
  7.2 17.2 %copy-start = (bf16[256,2048]{1,0:T(8,128)(2,1)S(1)}, bf16[256,2048]{1,0:T(8,128)(2,1)}, u32[]{:S(2)}) copy-start(bf16[256,2048]{1,0:T(8,128)(2,1)} %param.27) | copy-start | bytes 3145732
  14.5 9.8 %copy-start.1 = (bf16[32,2048]{1,0:T(8,128)(2,1)S(1)}, bf16[32,2048]{1,0:T(8,128)(2,1)}, u32[]{:S(2)}) copy-start(bf16[32,2048]{1,0:T(8,128)(2,1)} %param.20) | copy-start | bytes 393220
  14.5 9.8 %copy-start.2 = (bf16[2048,256]{1,0:T(8,128)(2,1)S(1)}, bf16[2048,256]{1,0:T(8,128)(2,1)}, u32[]{:S(2)}) copy-start(bf16[2048,256]{1,0:T(8,128)(2,1)} %param.25) | copy-start | bytes 3145732
  18.0 6.2 %copy-start.5 = (f32[32,2,128]{2,1,0:T(2,128)}, f32[32,2,128]{2,1,0:T(2,128)S(1)}, u32[]{:S(2)}) copy-start(f32[32,2,128]{2,1,0:T(2,128)S(1)} %reshape.238) | copy-start | bytes 98308
  18.4 5.9 %copy-start.7 = (f32[32,2,128]{2,1,0:T(2,128)}, f32[32,2,128]{2,1,0:T(2,128)S(1)}, u32[]{:S(2)}) copy-start(f32[32,2,128]{2,1,0:T(2,128)S(1)} %get-tuple-element.17) | copy-start | bytes 98308
  23.7 56.5 %copy-start.3 = (bf16[512,704]{0,1:T(8,128)(2,1)S(1)}, bf16[512,704]{0,1:T(8,128)(2,1)}, u32[]{:S(2)}) copy-start(bf16[512,704]{0,1:T(8,128)(2,1)} %param.33) | copy-start | bytes 2162692
  25.1 56.2 %copy-start.4 = (bf16[512,704]{0,1:T(8,128)(2,1)S(1)}, bf16[512,704]{0,1:T(8,128)(2,1)}, u32[]{:S(2)}) copy-start(bf16[512,704]{0,1:T(8,128)(2,1)} %param.32) | copy-start | bytes 2162692
  36.3 46.2 %all-to-all-start = ((bf16[8,16,2048]{2,1,0:T(8,128)(2,1)}), bf16[8,16,2048]{2,1,0:T(8,128)(2,1)S(1)}, u32[]{:S(2)}, u32[]{:S(2)}) async-start(bf16[8,16,2048]{2,1,0:T(8,128)(2,1)} %bitcast.5), calls=%async_computation | async-start | bytes 1048576 | tf_op jit(solution)/shard_map/all_to_all | solution.py:83
  42.1 71.8 %all-reduce.3.cloned.1.call-start = ((), (), s32[]{:S(2)}) async-start(), calls=%async_computation.6 | async-start | bytes 1441792 | tf_op jit(solution)/shard_map/psum | solution.py:171
  82.5 55.6 %reduce-scatter.3.cloned.1.call-start = ((), (), s32[]{:S(2)}) async-start(), calls=%async_computation.4 | async-start | bytes 655360 | tf_op jit(solution)/shard_map/reduce_scatter | solution.py:90
  85.4 5.7 %copy-start.10 = (s32[32,2]{0,1:T(2,128)S(1)}, s32[32,2]{0,1:T(2,128)}, u32[]{:S(2)}) copy-start(s32[32,2]{0,1:T(2,128)} %param.35) | copy-start | bytes 772
  85.5 5.9 %copy-start.6 = (f32[32,2,128]{2,1,0:T(2,128)S(1)}, f32[32,2,128]{2,1,0:T(2,128)}, u32[]{:S(2)}) copy-start(f32[32,2,128]{2,1,0:T(2,128)} %copy-done.5) | copy-start | bytes 98308
  85.5 5.9 %copy-start.8 = (f32[32,2,128]{2,1,0:T(2,128)S(1)}, f32[32,2,128]{2,1,0:T(2,128)}, u32[]{:S(2)}) copy-start(f32[32,2,128]{2,1,0:T(2,128)} %copy-done.7) | copy-start | bytes 98308
  91.1 112.4 %reduce-scatter.5.cloned.1.call-start = ((), (), s32[]{:S(2)}) async-start(), calls=%async_computation.5 | async-start | bytes 294912 | tf_op jit(solution)/shard_map/reduce_scatter | solution.py:174
  91.4 22.5 %copy-start.12 = (bf16[704,512]{1,0:T(8,128)(2,1)S(1)}, bf16[704,512]{1,0:T(8,128)(2,1)}, u32[]{:S(2)}) copy-start(bf16[704,512]{1,0:T(8,128)(2,1)} %param.34) | copy-start | bytes 2162692
  95.7 47.9 %copy-start.9 = (bf16[2048]{0:T(1024)(128)(2,1)S(1)}, bf16[2048]{0:T(1024)(128)(2,1)}, u32[]{:S(2)}) copy-start(bf16[2048]{0:T(1024)(128)(2,1)} %param.31) | copy-start | bytes 12292
  95.7 47.9 %copy-start.11 = (bf16[32,2]{0,1:T(2,128)(2,1)S(1)}, bf16[32,2]{0,1:T(2,128)(2,1)}, u32[]{:S(2)}) copy-start(bf16[32,2]{0,1:T(2,128)(2,1)} %param.36) | copy-start | bytes 388
  138.1 12.9 %all-to-all-start.1 = ((bf16[8,16,512]{2,1,0:T(8,128)(2,1)}), bf16[8,16,512]{2,1,0:T(8,128)(2,1)S(1)}, u32[]{:S(2)}, u32[]{:S(2)}) async-start(bf16[8,16,512]{2,1,0:T(8,128)(2,1)} %bitcast.75), calls=%async_computation.2 | async-start | bytes 262144 | tf_op jit(solution)/shard_map/all_to_all | solution.py:93
Sparse Core Ops, SparseCore 0:
  82.6 31.2 all-reduce.2
  116.4 21.6 reduce-scatter.2
  141.4 62.0 reduce-scatter.4
